TPU v7x, 32 devices: a whole 2x2x4 slice. The times are simulated.
32 devices in a mesh: ep: 8 (over z, y), tp: 4 (over x, core).
Axes of the slice: x: 2, y: 2, z: 4, core: 2. Of those that a mesh axis runs over, the one named last changes fastest.
Arguments:
- tokens: bfloat16 [6144, 2048], P('ep')
- in_gain: float32 [2048], replicated, may hold values from 0.1 to 1.9
- route_ids: int32 [6144, 2], P('ep'), may hold values from 0 to 7, all different within a row; in each aligned block of 768 rows (0 to 767, 768 to 1535, ...) at most 384 rows name the same one
- route_scores: float32 [6144, 2], P('ep'), may hold values from 0.1 to 1
- gate_weight: bfloat16 [8, 2048, 1024], P('ep', None, 'tp'), may hold values from -0.125 to 0.125
- up_weight: bfloat16 [8, 2048, 1024], P('ep', None, 'tp'), may hold values from -0.125 to 0.125
- down_weight: bfloat16 [8, 1024, 2048], P('ep', 'tp')
- out_gain: float32 [2048], P('tp'), may hold values from 0.1 to 1.9
Outputs:
- mixed: bfloat16 [6144, 2048], P('ep', 'tp')
Inputs may be any that keep to these rules, and one draw needn't show every extreme that they name: `route_ids`: each row names 2 different experts. Among the rows of one index of ep (aligned blocks of 768 rows) no expert is named more than 384 times, a bound that some block reaches.
All inputs are finite; a program needn't handle non-finite values.
Results may differ from a plain program's by a relative error of at most 0.012.
Values may be sent and summed in bfloat16 or wider, within the bound.
A program may use at most 128 MiB of HBM per device.

v0:
```python
import jax
import jax.numpy as jnp
from jax import lax
from jax.sharding import PartitionSpec as P

epsilon = 1e-06


def per_device(
    tokens, in_gain, route_ids, route_scores, gate_weight, up_weight, down_weight, out_gain
):
    count_ep = lax.axis_size("ep")
    count_tp = lax.axis_size("tp")
    local_experts = gate_weight.shape[0]
    experts = count_ep * local_experts
    tok_count, full_width = tokens.shape
    choose_count = route_ids.shape[1]
    capacity = 2 * tok_count * choose_count // experts
    part_width = full_width // count_tp
    as_float = tokens.astype(jnp.float32)
    normed = (
        as_float
        * lax.rsqrt(jnp.mean(as_float * as_float, axis=1, keepdims=True) + epsilon)
        * in_gain
    ).astype(jnp.bfloat16)
    flat_ids = route_ids.reshape(-1)
    one_hot = (flat_ids[:, None] == jnp.arange(experts, dtype=jnp.int32)[None, :]).astype(jnp.int32)
    slot_index = jnp.sum((jnp.cumsum(one_hot, axis=0) - 1) * one_hot, axis=1)
    row_index = jnp.arange(tok_count * choose_count, dtype=jnp.int32) // choose_count
    own_slice = lax.dynamic_slice_in_dim(normed, lax.axis_index("tp") * part_width, part_width, 1)
    buffer = jnp.zeros((experts, capacity, part_width), jnp.bfloat16)
    buffer = buffer.at[flat_ids, slot_index].set(own_slice[row_index])
    buffer = buffer.reshape(count_ep, local_experts, capacity, part_width)
    received = lax.all_to_all(buffer, "ep", split_axis=0, concat_axis=0, tiled=True)
    piece = lax.all_gather(received, "tp", axis=3, tiled=True)
    gate_add = jnp.einsum("secn,enf->secf", piece, gate_weight, preferred_element_type=jnp.float32)
    up_add = jnp.einsum("secn,enf->secf", piece, up_weight, preferred_element_type=jnp.float32)
    hidden = (jax.nn.silu(gate_add) * up_add).astype(jnp.bfloat16)
    partial_terms = jnp.einsum(
        "secf,efd->secd", hidden, down_weight, preferred_element_type=jnp.float32
    ).astype(jnp.bfloat16)
    summed = (
        lax.psum_scatter(partial_terms, "tp", scatter_dimension=3, tiled=True)
        .astype(jnp.float32)
        .astype(jnp.bfloat16)
    )
    returned = lax.all_to_all(summed, "ep", split_axis=0, concat_axis=0, tiled=True).reshape(
        experts, capacity, part_width
    )
    picked = (
        returned[flat_ids, slot_index]
        .astype(jnp.float32)
        .reshape(tok_count, choose_count, part_width)
    )
    mix_weight = route_scores / jnp.sum(route_scores, axis=1, keepdims=True)
    combined = jnp.sum(mix_weight[:, :, None] * picked, axis=1)
    squares_sum = lax.psum(jnp.sum(combined * combined, axis=1), "tp")
    scaled = combined * lax.rsqrt(squares_sum[:, None] / full_width + epsilon) * out_gain
    return scaled.astype(jnp.bfloat16)


def solution(mesh):
    in_specs = (
        P("ep", None),
        P(),
        P("ep", None),
        P("ep", None),
        P("ep", None, "tp"),
        P("ep", None, "tp"),
        P("ep", "tp", None),
        P("tp"),
    )
    out_specs = P("ep", "tp")
    return jax.shard_map(
        per_device, mesh=mesh, in_specs=in_specs, out_specs=out_specs, check_vma=False
    )
```

profile of v0, /device:TPU:0, one launch (start us, length us, event | category | flops | bytes accessed | tf_op | source)
XLA Modules:
  0.0 441.9 jit_solution(14998475770619304312)
XLA Ops:
  6.5 1.0 copy.15
  7.5 0.2 eq.29
  7.7 0.2 eq.25
  8.0 0.2 reshape.152
  8.2 5.5 %convert_element_type.39 = f32[768,2048]{1,0:T(8,128)} convert(bf16[768,2048]{1,0:T(8,128)(2,1)} %param.8) | non-fusion elementwise | flops 1572864 | bytes 9437184 | tf_op jit(solution)/shard_map/convert_element_type | solution.py:20
  13.8 0.7 multiply_reduce_fusion
  14.5 0.1 fusion.27
  14.5 2.3 reduce-window.6
  16.8 0.3 slice_reduce_fusion
  17.1 0.2 reduce-window.9
  17.3 0.1 add_bitcast_fusion
  17.5 0.1 multiply_reduce_fusion.3
  17.6 0.1 and_reduce_fusion
  17.7 0.8 dynamic-slice
  18.5 1.6 fusion.11
  20.1 16.3 %scatter_custom_fusion = bf16[3072,512]{1,0:T(8,128)(2,1)} fusion(s32[1536]{0:T(1024)S(1)} %broadcast_select_fusion, bf16[768,512]{1,0:T(8,128)(2,1)S(1)} %fusion.11, s32[2048]{0:T(1024)S(1)} %pad_clamp_fusion, bf16[]{:T(256)} %constant.38.clone.1), kind=kCustom, calls=%fused_computation.21 | custom fusion | bytes 3145730
  36.4 78.1 %all_to_all.10 = bf16[8,1,384,512]{3,2,1,0:T(8,128)(2,1)} all-to-all(bf16[8,1,384,512]{3,2,1,0:T(8,128)(2,1)} %bitcast.86), channel_id=1, replica_groups=mesh['ep'=8,'tp'=4] {'ep'}, dimensions={0} | all-to-all | bytes 6291456 | tf_op jit(solution)/shard_map/all_to_all | solution.py:34
  114.5 0.0 all-gather.2.cloned.1.call-update
  114.6 0.2 reduce-scatter.2.cloned.1.call-start
  114.8 81.0 %all-gather.2.cloned.1.call-done = bf16[8,1,384,2048]{3,2,0,1:T(8,128)(2,1)} async-done(((bf16[8,1,384,512]{3,2,0,1:T(8,128)(2,1)}), bf16[8,1,384,2048]{3,2,0,1:T(8,128)(2,1)}) %all-gather.2.cloned.1.call-update) | async-done | bytes 12582928 | tf_op jit(solution)/shard_map/all_gather | solution.py:35
  195.8 9.8 %fusion.2 = f32[8,384,256]{2,1,0:T(8,128)} fusion(bf16[8,1,384,2048]{3,2,0,1:T(8,128)(2,1)} %all-gather.2.cloned.1.call-done, bf16[1,2048,256]{2,1,0:T(8,128)(2,1)S(1)} %copy-done.6), kind=kOutput, calls=%fused_computation.5 | convolution fusion | flops 3221225472 | bytes 16777216 | tf_op jit(solution)/shard_map/secn,enf->secf/dot_general | solution.py:36
  205.6 18.8 %convert_bitcast_fusion = bf16[8,1,384,2048]{3,2,0,1:T(8,128)(2,1)} fusion(f32[8,384,256]{2,1,0:T(8,128)} %fusion.2, bf16[8,1,384,2048]{3,2,0,1:T(8,128)(2,1)} %all-gather.2.cloned.1.call-done, bf16[1,256,2048]{2,1,0:T(8,128)(2,1)S(1)} %copy-done, bf16[1,2048,256]{2,1,0:T(8,128)(2,1)S(1)} %copy-done.7), kind=kOutput, calls=%fused_computation.7 | convolution fusion | flops 6453460992 | bytes 30408704 | tf_op jit(solution)/shard_map/secf,efd->secd/dot_general | solution.py:39
  224.4 97.3 %reduce-scatter.2.cloned.1.call-done = bf16[8,1,384,512]{3,2,0,1:T(8,128)(2,1)} async-done(((bf16[8,1,384,2048]{3,2,0,1:T(8,128)(2,1)}), bf16[8,1,384,512]{3,2,0,1:T(8,128)(2,1)}) %reduce-scatter.2.cloned.1.call-update) | async-done | bytes 3145744 | tf_op jit(solution)/shard_map/reduce_scatter | solution.py:43
  321.7 5.6 %all-to-all-start.1 = ((bf16[8,1,384,512]{3,2,1,0:T(8,128)(2,1)}), bf16[8,1,384,512]{3,2,1,0:T(8,128)(2,1)}, u32[]{:S(2)}, u32[]{:S(2)}) async-start(bf16[8,1,384,512]{3,2,1,0:T(8,128)(2,1)} %bitcast.87), calls=%async_computation.2 | async-start | bytes 6291456 | tf_op jit(solution)/shard_map/all_to_all | solution.py:47
  327.4 0.2 copy.14
  327.6 70.4 %all-to-all-done.1 = bf16[8,1,384,512]{3,2,1,0:T(8,128)(2,1)} async-done(((bf16[8,1,384,512]{3,2,1,0:T(8,128)(2,1)}), bf16[8,1,384,512]{3,2,1,0:T(8,128)(2,1)}, u32[]{:S(2)}, u32[]{:S(2)}) %all-to-all-start.1) | async-done | bytes 3145760 | tf_op jit(solution)/shard_map/all_to_all | solution.py:47
  398.0 20.5 %gather_fusion = bf16[1536,512]{1,0:T(8,128)(2,1)S(1)} fusion(bf16[8,384,512]{2,1,0:T(8,128)(2,1)} %bitcast.23, s32[1536]{0:T(1024)S(1)} %get-tuple-element.5), kind=kCustom, calls=%fused_computation.1 | custom fusion | bytes 3158016 | tf_op jit(solution)/shard_map/gather | solution.py:51
  418.5 3.3 reshape.166
  421.8 6.0 %multiply_reduce_fusion.1 = f32[768,512]{1,0:T(8,128)S(1)} fusion(f32[768,2,512]{2,1,0:T(2,128)} %reshape.166, f32[768,2]{1,0:T(8,128)S(1)} %copy.14), kind=kLoop, calls=%fused_computation.16 | loop fusion | flops 1179648 | bytes 4724736 | tf_op jit(solution)/shard_map/reduce_sum | solution.py:56
  427.8 0.2 multiply_reduce_fusion.2
  428.0 6.0 %psum.7 = f32[768]{0:T(1024)S(1)} all-reduce(f32[768]{0:T(1024)S(1)} %multiply_reduce_fusion.2), channel_id=1, replica_groups=mesh['ep'=8,'tp'=4] {'tp'}, use_global_device_ids=true, to_apply=%region_9.10 | all-reduce | flops 768 | bytes 6144 | tf_op jit(solution)/shard_map/psum | solution.py:57
  434.0 1.1 multiply_convert_fusion
  (27 shorter events, 0.2 us)
Async XLA Ops:
  6.5 199.1 %copy-start = (bf16[1,256,2048]{2,1,0:T(8,128)(2,1)S(1)}, bf16[1,256,2048]{2,1,0:T(8,128)(2,1)}, u32[]{:S(2)}) copy-start(bf16[1,256,2048]{2,1,0:T(8,128)(2,1)} %param.14) | copy-start | bytes 3145732
  6.5 189.3 %all-gather.2.cloned.1.call-start = ((), (), s32[]{:S(2)}) async-start(), calls=%async_computation.3 | async-start | bytes 15728640 | tf_op jit(solution)/shard_map/all_gather | solution.py:35
  8.2 5.6 %copy-start.1 = (bf16[768,2048]{1,0:T(8,128)(2,1)S(1)}, bf16[768,2048]{1,0:T(8,128)(2,1)}, u32[]{:S(2)}) copy-start(bf16[768,2048]{1,0:T(8,128)(2,1)} %param.8) | copy-start | bytes 9437188
  13.8 3.7 copy-start.5
  13.8 3.8 copy-start.4
  114.5 81.3 %copy-start.6 = (bf16[1,2048,256]{2,1,0:T(8,128)(2,1)S(1)}, bf16[1,2048,256]{2,1,0:T(8,128)(2,1)}, u32[]{:S(2)}) copy-start(bf16[1,2048,256]{2,1,0:T(8,128)(2,1)} %param.12) | copy-start | bytes 3145732
  114.6 91.0 %copy-start.7 = (bf16[1,2048,256]{2,1,0:T(8,128)(2,1)S(1)}, bf16[1,2048,256]{2,1,0:T(8,128)(2,1)}, u32[]{:S(2)}) copy-start(bf16[1,2048,256]{2,1,0:T(8,128)(2,1)} %param.13) | copy-start | bytes 3145732
  114.6 207.2 %reduce-scatter.2.cloned.1.call-start = ((), (), s32[]{:S(2)}) async-start(), calls=%async_computation.4 | async-start | bytes 15728640 | tf_op jit(solution)/shard_map/reduce_scatter | solution.py:43
  321.7 5.6 %copy-start.2 = (f32[768,2]{0,1:T(2,128)S(1)}, f32[768,2]{0,1:T(2,128)}, u32[]{:S(2)}) copy-start(f32[768,2]{0,1:T(2,128)} %param.11) | copy-start | bytes 18436
  321.7 76.3 %all-to-all-start.1 = ((bf16[8,1,384,512]{3,2,1,0:T(8,128)(2,1)}), bf16[8,1,384,512]{3,2,1,0:T(8,128)(2,1)}, u32[]{:S(2)}, u32[]{:S(2)}) async-start(bf16[8,1,384,512]{3,2,1,0:T(8,128)(2,1)} %bitcast.87), calls=%async_computation.2 | async-start | bytes 6291456 | tf_op jit(solution)/shard_map/all_to_all | solution.py:47
  421.8 12.2 %copy-start.3 = (f32[512]{0:T(512)S(1)}, f32[512]{0:T(512)}, u32[]{:S(2)}) copy-start(f32[512]{0:T(512)} %param.15) | copy-start | bytes 6148
Sparse Core Ops, SparseCore 0:
  114.7 81.0 all-gather.1
  224.5 97.1 reduce-scatter.1
where the time goes:
time: 443 us; the launch traced here: 442 us
  waiting for transfers between devices  249 us (56%)
  blocking collectives  84.1 us (19%)
  local copies, waits for them, and re-layouts  43 us (10%)
  matrix products  28.6 us (6%)
  other arithmetic  18 us (4%)
  between operations  13.6 us (3%)
  starting transfers between devices  5.85 us (1%)
    reduce_scatter x1, waiting for transfers between devices, per_device(): lax.psum_scatter(partial_terms, 'tp', scatter_dimension=3, tiled=True)  97.3 us
    all_gather x1, waiting for transfers between devices, per_device(): piece = lax.all_gather(received, 'tp', axis=3, tiled=True)  81 us
    all_to_all x1, blocking collectives, per_device(): lax.all_to_all(buffer, 'ep', split_axis=0, concat_axis=0, tiled=True)  78.1 us
    all_to_all x1, waiting for transfers between devices, per_device(): lax.all_to_all(summed, 'ep', split_axis=0, concat_axis=0, tiled=True)  70.4 us
    gather x1, local copies, waits for them, and re-layouts, per_device(): returned[flat_ids, slot_index].astype(jnp.float32)  20.5 us
    dot_general x1, matrix products, per_device(): jnp.einsum('secf,efd->secd', hidden, down_weight, preferred_element_type=...  18.8 us
    unnamed x18, local copies, waits for them, and re-layouts  17.3 us
    dot_general x1, matrix products, per_device(): jnp.einsum('secn,enf->secf', piece, gate_weight, preferred_element_type=j...  9.79 us
  transfers between devices with their start and end apart: 3, of which 3 were waited for; matrix products, arithmetic and copies ran while one was open for 0% of the time, Pallas kernels for 0%

commit v1 on v0

--- a/solution.py
+++ b/solution.py
@@ -32,7 +32,7 @@
     buffer = buffer.at[flat_ids, slot_index].set(own_slice[row_index])
     buffer = buffer.reshape(count_ep, local_experts, capacity, part_width)
     received = lax.all_to_all(buffer, "ep", split_axis=0, concat_axis=0, tiled=True)
-    piece = lax.all_gather(received, "tp", axis=3, tiled=True)
+    piece = jnp.concatenate(lax.all_gather(received, "tp"), axis=3)
     gate_add = jnp.einsum("secn,enf->secf", piece, gate_weight, preferred_element_type=jnp.float32)
     up_add = jnp.einsum("secn,enf->secf", piece, up_weight, preferred_element_type=jnp.float32)
     hidden = (jax.nn.silu(gate_add) * up_add).astype(jnp.bfloat16)

time: 443 us -> 479 us (1.081)
  local copies, waits for them, and re-layouts: 43 us -> 78.7 us
    another operation x0 -> x1, local copies, waits for them, and re-layouts: none -> 21 us
    reshape x0 -> x1, local copies, waits for them, and re-layouts: none -> 15.6 us  [per_device(): piece = jnp.concatenate(lax.all_gather(received, 'tp'), axis=3)]
    unnamed x18 -> x20, local copies, waits for them, and re-layouts: 17.3 us -> 17.3 us
where the time goes in v1:
time: 479 us; the launch traced here: 478 us
  waiting for transfers between devices  249 us (52%)
  blocking collectives  84.1 us (18%)
  local copies, waits for them, and re-layouts  78.7 us (16%)
  matrix products  28.7 us (6%)
  other arithmetic  18.1 us (4%)
  between operations  13.6 us (3%)
  starting transfers between devices  5.87 us (1%)
    reduce_scatter x1, waiting for transfers between devices, per_device(): lax.psum_scatter(partial_terms, 'tp', scatter_dimension=3, tiled=True)  97.3 us
    all_gather x1, waiting for transfers between devices, per_device(): piece = jnp.concatenate(lax.all_gather(received, 'tp'), axis=3)  81 us
    all_to_all x1, blocking collectives, per_device(): lax.all_to_all(buffer, 'ep', split_axis=0, concat_axis=0, tiled=True)  78.1 us
    all_to_all x1, waiting for transfers between devices, per_device(): lax.all_to_all(summed, 'ep', split_axis=0, concat_axis=0, tiled=True)  70.3 us
    another operation x1, local copies, waits for them, and re-layouts  21 us
    dot_general x1, matrix products, per_device(): jnp.einsum('secf,efd->secd', hidden, down_weight, preferred_element_type=...  18.8 us
    gather x1, local copies, waits for them, and re-layouts, per_device(): returned[flat_ids, slot_index].astype(jnp.float32)  18 us
    unnamed x20, local copies, waits for them, and re-layouts  17.3 us
  transfers between devices with their start and end apart: 3, of which 3 were waited for; matrix products, arithmetic and copies ran while one was open for 0% of the time, Pallas kernels for 0%

profile of v1, /device:TPU:0, one launch (start us, length us, event | category | flops | bytes accessed | tf_op | source)
XLA Modules:
  0.0 477.6 jit_solution(2302486951629735300)
XLA Ops:
  6.5 1.0 copy.16
  7.5 0.2 eq.29
  7.7 0.2 eq.25
  8.0 0.2 reshape.158
  8.2 5.5 %convert_element_type.39 = f32[768,2048]{1,0:T(8,128)} convert(bf16[768,2048]{1,0:T(8,128)(2,1)} %param.8) | non-fusion elementwise | flops 1572864 | bytes 9437184 | tf_op jit(solution)/shard_map/convert_element_type | solution.py:20
  13.8 0.7 multiply_reduce_fusion
  14.5 2.3 reduce-window.6
  16.8 0.3 slice_reduce_fusion
  17.1 0.2 reduce-window.9
  17.3 0.1 add_bitcast_fusion
  17.5 0.1 multiply_reduce_fusion.3
  17.6 0.1 and_reduce_fusion
  17.7 0.8 dynamic-slice
  18.5 1.6 fusion.5
  20.1 16.3 %scatter_custom_fusion = bf16[3072,512]{1,0:T(8,128)(2,1)} fusion(s32[1536]{0:T(1024)S(1)} %broadcast_select_fusion, bf16[768,512]{1,0:T(8,128)(2,1)S(1)} %fusion.5, s32[2048]{0:T(1024)S(1)} %pad_clamp_fusion, bf16[]{:T(256)} %constant.38.clone.1), kind=kCustom, calls=%fused_computation.17 | custom fusion | bytes 3145730
  36.4 78.1 %all_to_all.10 = bf16[8,1,384,512]{3,2,1,0:T(8,128)(2,1)} all-to-all(bf16[8,1,384,512]{3,2,1,0:T(8,128)(2,1)} %bitcast.85), channel_id=1, replica_groups=mesh['ep'=8,'tp'=4] {'ep'}, dimensions={0} | all-to-all | bytes 6291456 | tf_op jit(solution)/shard_map/all_to_all | solution.py:34
  114.6 0.2 reduce-scatter.2.cloned.1.call-start
  114.8 81.0 %all-gather.3.cloned.1.call-done = bf16[32,1,384,512]{3,2,1,0:T(8,128)(2,1)} async-done(((bf16[8,1,384,512]{3,2,1,0:T(8,128)(2,1)}), bf16[32,1,384,512]{3,2,1,0:T(8,128)(2,1)}) %all-gather.3.cloned.1.call-update) | async-done | bytes 12582928 | tf_op jit(solution)/shard_map/all_gather | solution.py:35
  195.8 15.6 %copy.19 = bf16[8,1,384,4,512]{4,3,2,0,1:T(4,128)(2,1)} copy(bf16[8,1,384,4,512]{4,2,0,3,1:T(8,128)(2,1)} %bitcast.84) | data formatting | bytes 25165824 | tf_op jit(solution)/shard_map/reshape | solution.py:35
  211.4 21.0 %reshape.162 = bf16[8,384,2048]{2,1,0:T(8,128)(2,1)} reshape(bf16[8,1,384,4,512]{4,3,2,0,1:T(4,128)(2,1)} %copy.19) | data formatting | bytes 25165824 | tf_op jit(solution)/shard_map/reshape.4
  232.4 9.9 %fusion.11 = f32[8,384,256]{2,1,0:T(8,128)} fusion(bf16[8,384,2048]{2,1,0:T(8,128)(2,1)} %reshape.162, bf16[1,2048,256]{2,1,0:T(8,128)(2,1)S(1)} %copy-done.7), kind=kOutput, calls=%fused_computation.23 | convolution fusion | flops 3221225472 | bytes 16777216 | tf_op jit(solution)/shard_map/secn,enf->secf/dot_general | solution.py:37
  242.3 18.8 %convert_bitcast_fusion = bf16[8,1,384,2048]{3,2,0,1:T(8,128)(2,1)} fusion(bf16[1,256,2048]{2,1,0:T(8,128)(2,1)S(1)} %copy-done, f32[8,384,256]{2,1,0:T(8,128)} %fusion.11, bf16[8,384,2048]{2,1,0:T(8,128)(2,1)} %reshape.162, bf16[1,2048,256]{2,1,0:T(8,128)(2,1)S(1)} %copy-done.8), kind=kOutput, calls=%fused_computation.3 | convolution fusion | flops 6453460992 | bytes 30408704 | tf_op jit(solution)/shard_map/secf,efd->secd/dot_general | solution.py:39
  261.2 97.3 %reduce-scatter.2.cloned.1.call-done = bf16[8,1,384,512]{3,2,0,1:T(8,128)(2,1)} async-done(((bf16[8,1,384,2048]{3,2,0,1:T(8,128)(2,1)}), bf16[8,1,384,512]{3,2,0,1:T(8,128)(2,1)}) %reduce-scatter.2.cloned.1.call-update) | async-done | bytes 3145744 | tf_op jit(solution)/shard_map/reduce_scatter | solution.py:43
  358.4 5.6 %all-to-all-start.1 = ((bf16[8,1,384,512]{3,2,1,0:T(8,128)(2,1)}), bf16[8,1,384,512]{3,2,1,0:T(8,128)(2,1)S(1)}, u32[]{:S(2)}, u32[]{:S(2)}) async-start(bf16[8,1,384,512]{3,2,1,0:T(8,128)(2,1)} %bitcast.86), calls=%async_computation.2 | async-start | bytes 6291456 | tf_op jit(solution)/shard_map/all_to_all | solution.py:47
  364.1 0.2 copy.15
  364.3 70.3 %all-to-all-done.1 = bf16[8,1,384,512]{3,2,1,0:T(8,128)(2,1)S(1)} async-done(((bf16[8,1,384,512]{3,2,1,0:T(8,128)(2,1)}), bf16[8,1,384,512]{3,2,1,0:T(8,128)(2,1)S(1)}, u32[]{:S(2)}, u32[]{:S(2)}) %all-to-all-start.1) | async-done | bytes 3145760 | tf_op jit(solution)/shard_map/all_to_all | solution.py:47
  434.7 18.0 %gather_fusion = bf16[1536,512]{1,0:T(8,128)(2,1)} fusion(bf16[8,384,512]{2,1,0:T(8,128)(2,1)S(1)} %bitcast.83, s32[1536]{0:T(1024)S(1)} %get-tuple-element.5), kind=kCustom, calls=%fused_computation.1 | custom fusion | bytes 3158016 | tf_op jit(solution)/shard_map/gather | solution.py:51
  452.7 4.7 reshape.173
  457.4 6.1 %multiply_reduce_fusion.1 = f32[768,512]{1,0:T(8,128)S(1)} fusion(f32[768,2,512]{2,1,0:T(2,128)} %reshape.173, f32[768,2]{1,0:T(8,128)S(1)} %copy.15), kind=kLoop, calls=%fused_computation.12 | loop fusion | flops 1179648 | bytes 4724736 | tf_op jit(solution)/shard_map/reduce_sum | solution.py:56
  463.5 0.2 multiply_reduce_fusion.2
  463.7 6.0 %psum.7 = f32[768]{0:T(1024)S(1)} all-reduce(f32[768]{0:T(1024)S(1)} %multiply_reduce_fusion.2), channel_id=1, replica_groups=mesh['ep'=8,'tp'=4] {'tp'}, use_global_device_ids=true, to_apply=%region_9.10 | all-reduce | flops 768 | bytes 6144 | tf_op jit(solution)/shard_map/psum | solution.py:57
  469.7 1.1 multiply_convert_fusion
  (31 shorter events, 0.3 us)
Async XLA Ops:
  6.5 235.8 %copy-start = (bf16[1,256,2048]{2,1,0:T(8,128)(2,1)S(1)}, bf16[1,256,2048]{2,1,0:T(8,128)(2,1)}, u32[]{:S(2)}) copy-start(bf16[1,256,2048]{2,1,0:T(8,128)(2,1)} %param.14) | copy-start | bytes 3145732
  6.5 189.3 %all-gather.3.cloned.1.call-start = ((), (), s32[]{:S(2)}) async-start(), calls=%async_computation.4 | async-start | bytes 15728640 | tf_op jit(solution)/shard_map/all_gather | solution.py:35
  8.2 5.6 %copy-start.2 = (bf16[768,2048]{1,0:T(8,128)(2,1)S(1)}, bf16[768,2048]{1,0:T(8,128)(2,1)}, u32[]{:S(2)}) copy-start(bf16[768,2048]{1,0:T(8,128)(2,1)} %param.8) | copy-start | bytes 9437188
  13.8 3.7 copy-start.6
  13.8 3.8 copy-start.5
  114.6 243.9 %reduce-scatter.2.cloned.1.call-start = ((), (), s32[]{:S(2)}) async-start(), calls=%async_computation.3 | async-start | bytes 15728640 | tf_op jit(solution)/shard_map/reduce_scatter | solution.py:43
  211.4 21.0 %copy-start.7 = (bf16[1,2048,256]{2,1,0:T(8,128)(2,1)S(1)}, bf16[1,2048,256]{2,1,0:T(8,128)(2,1)}, u32[]{:S(2)}) copy-start(bf16[1,2048,256]{2,1,0:T(8,128)(2,1)} %param.13) | copy-start | bytes 3145732
  232.4 9.9 %copy-start.8 = (bf16[1,2048,256]{2,1,0:T(8,128)(2,1)S(1)}, bf16[1,2048,256]{2,1,0:T(8,128)(2,1)}, u32[]{:S(2)}) copy-start(bf16[1,2048,256]{2,1,0:T(8,128)(2,1)} %param.12) | copy-start | bytes 3145732
  358.4 5.7 %copy-start.3 = (f32[768,2]{0,1:T(2,128)S(1)}, f32[768,2]{0,1:T(2,128)}, u32[]{:S(2)}) copy-start(f32[768,2]{0,1:T(2,128)} %param.11) | copy-start | bytes 18436
  358.4 76.2 %all-to-all-start.1 = ((bf16[8,1,384,512]{3,2,1,0:T(8,128)(2,1)}), bf16[8,1,384,512]{3,2,1,0:T(8,128)(2,1)S(1)}, u32[]{:S(2)}, u32[]{:S(2)}) async-start(bf16[8,1,384,512]{3,2,1,0:T(8,128)(2,1)} %bitcast.86), calls=%async_computation.2 | async-start | bytes 6291456 | tf_op jit(solution)/shard_map/all_to_all | solution.py:47
  457.4 12.2 %copy-start.4 = (f32[512]{0:T(512)S(1)}, f32[512]{0:T(512)}, u32[]{:S(2)}) copy-start(f32[512]{0:T(512)} %param.15) | copy-start | bytes 6148
  457.4 13.3 %copy-start.1 = (bf16[1,256,2048]{2,1,0:T(8,128)(2,1)S(1)}, bf16[1,256,2048]{2,1,0:T(8,128)(2,1)}, u32[]{:S(2)}) copy-start(bf16[1,256,2048]{2,1,0:T(8,128)(2,1)} %param.14) | copy-start | bytes 3145732
Sparse Core Ops, SparseCore 0:
  114.7 81.0 all-gather.2
  261.3 97.1 reduce-scatter.1
